TPU v7x, 32 devices: a whole 2x2x4 slice. The times are simulated.
32 devices in a mesh: ep: 8 (over z, x), tp: 4 (over y, core).
Axes of the slice: x: 2, y: 2, z: 4, core: 2. Of those that a mesh axis runs over, the one named last changes fastest.
Arguments:
- mix_input: bfloat16 [3072, 2048], P('ep', 'tp'), may hold values from -6 to 6
- mix_gain: float32 [2048], replicated, may hold values from 0.1 to 1.9
- gate_b_weight: bfloat16 [2048, 2048], P(None, 'tp'), may hold values from -0.125 to 0.125
- gate_c_weight: bfloat16 [2048, 2048], P(None, 'tp'), may hold values from -0.125 to 0.125
- value_weight: bfloat16 [2048, 2048], P(None, 'tp'), may hold values from -0.125 to 0.125
- conv_weight: float32 [3, 2048], P(None, 'tp'), may hold values from -3 to 3
- out_weight: bfloat16 [2048, 2048], P('tp'), may hold values from -0.125 to 0.125
- expert_input: bfloat16 [1280, 2048], P('ep', 'tp'), may hold values from -6 to 6
- expert_gain: float32 [2048], replicated, may hold values from 0.1 to 1.9
- routes: int32 [1280, 2], P('ep'), may hold values from 0 to 7, all different within a row; in each aligned block of 160 rows (0 to 159, 160 to 319, ...) at most 80 rows name the same one
- route_weight: float32 [1280, 2], P('ep'), may hold values from 0.2 to 1
- expert_gate: bfloat16 [8, 2048, 3072], P('ep', None, 'tp'), may hold values from -0.125 to 0.125
- expert_up: bfloat16 [8, 2048, 3072], P('ep', None, 'tp'), may hold values from -0.125 to 0.125
- expert_down: bfloat16 [8, 3072, 2048], P('ep', 'tp'), may hold values from -0.109375 to 0.109375
Outputs:
- mix_output: bfloat16 [3072, 2048], P('ep', 'tp')
- expert_output: bfloat16 [1280, 2048], P('ep', 'tp')
Inputs may be any that keep to these rules, and one draw needn't show every extreme that they name: `routes`: the 2 experts of a row differ. Among the rows of one device no expert is named more than 80 times, a bound that some block reaches.
All inputs are finite; a program needn't handle non-finite values.
Results may differ from a plain program's by a relative error of at most 0.019.
Values may be sent and summed in bfloat16 or wider, within the bound.
No kernel may reach another device: no remote copies, remote signals or barrier semaphores. Data moves between devices by JAX's collectives and lax.ppermute only.
A program may use at most 64 MiB of HBM per device.

v0:
```python
import jax
import jax.numpy as jnp
from jax import lax
from jax.sharding import PartitionSpec as P

epsilon = 1e-06
routed_scale = 2.5


def passed_along(block, axis, distance):
    devices = range(lax.axis_size(axis))
    route = [(i - distance, i) for i in devices if i - distance in devices]
    return lax.ppermute(block, axis, route)


def project_piece(piece, gain_vector, matrices, group_count):
    widened = piece.astype(jnp.float32)
    columns = piece.shape[-1]
    scaled = (widened * gain_vector).astype(jnp.bfloat16)
    grouped = scaled.reshape(group_count, -1, columns)
    updated = tuple(
        (
            jnp.einsum("gsd,gdf->gsf", grouped, matrix, preferred_element_type=jnp.float32)
            for matrix in matrices
        )
    )
    return (updated, jnp.sum(widened * widened, axis=-1))


def local(
    mix_input,
    mix_gain,
    gate_b_weight,
    gate_c_weight,
    value_weight,
    conv_weight,
    out_weight,
    expert_input,
    expert_gain,
    routes,
    route_weight,
    expert_gate,
    expert_up,
    expert_down,
):
    ep_count = lax.axis_size("ep")
    local_experts = expert_gate.shape[0]
    model_width = mix_gain.shape[0]
    expert_count = local_experts * ep_count
    tok_local, top_count = routes.shape
    capacity = 2 * tok_local * top_count // expert_count
    feature_local = expert_input.shape[1]
    mix_rows = mix_input.shape[0]
    slot_rows = ep_count * capacity
    flat_routes = routes.reshape(-1)
    pair_count = flat_routes.shape[0]
    matches = (
        flat_routes[:, None] == lax.broadcasted_iota(jnp.int32, (pair_count, expert_count), 1)
    ).astype(jnp.int32)
    ranks = jnp.sum((jnp.cumsum(matches, axis=0) - matches) * matches, axis=1)
    slot_iota = lax.broadcasted_iota(jnp.int32, (pair_count, expert_count * capacity), 1)
    send_table = (slot_iota == (flat_routes * capacity + ranks)[:, None]).astype(jnp.bfloat16)
    back_index = (
        flat_routes % local_experts * slot_rows + flat_routes // local_experts * capacity + ranks
    )
    back_table = (slot_iota == back_index[:, None]).astype(jnp.bfloat16)
    repeated = jnp.repeat(expert_input, top_count, axis=0)
    outgoing = lax.dot_general(
        send_table, repeated, (((0,), (0,)), ((), ())), preferred_element_type=jnp.float32
    ).astype(jnp.bfloat16)
    outgoing = outgoing.reshape(ep_count, local_experts, capacity, feature_local)
    arrived = lax.all_to_all(outgoing, "ep", split_axis=0, concat_axis=2, tiled=True)
    arrived = arrived.reshape(local_experts * slot_rows, feature_local)
    mix_weights = (gate_b_weight[None], gate_c_weight[None], value_weight[None])
    expert_weights = (expert_gate, expert_up)
    mix_carry = project_piece(
        lax.all_gather(mix_input, "tp", axis=1, tiled=True), mix_gain, mix_weights, 1
    )
    expert_carry = project_piece(
        lax.all_gather(arrived, "tp", axis=1, tiled=True),
        expert_gain,
        expert_weights,
        local_experts,
    )
    mix_totals, mix_squares = mix_carry
    mix_factor = lax.rsqrt(mix_squares / model_width + epsilon)[:, None]
    outer_gate = mix_totals[0][0] * mix_factor
    product = mix_totals[1][0] * mix_factor * (mix_totals[2][0] * mix_factor)
    edge_rows = passed_along(product[mix_rows - 2 :], "ep", 1)
    padded = jnp.concatenate([edge_rows, product], axis=0)
    convolved = (
        conv_weight[0] * padded[:mix_rows]
        + conv_weight[1] * padded[1 : mix_rows + 1]
        + conv_weight[2] * padded[2:]
    )
    gated = (outer_gate * convolved).astype(jnp.bfloat16)
    expert_totals, expert_squares = expert_carry
    expert_factor = lax.rsqrt(expert_squares / model_width + epsilon).reshape(
        local_experts, slot_rows, 1
    )
    activated = (
        jax.nn.silu(expert_totals[0] * expert_factor) * (expert_totals[1] * expert_factor)
    ).astype(jnp.bfloat16)
    sliced = out_weight
    mix_sum = lax.psum_scatter(
        lax.dot_general(
            sliced, gated, (((0,), (1,)), ((), ())), preferred_element_type=jnp.float32
        ).astype(jnp.bfloat16),
        "tp",
        scatter_dimension=0,
        tiled=True,
    ).astype(jnp.float32)
    sliced = expert_down
    summed = jnp.einsum("gsf,gfd->dgs", activated, sliced, preferred_element_type=jnp.float32)
    expert_sum = lax.psum_scatter(
        summed.reshape(lax.axis_size("tp") * feature_local, local_experts * slot_rows).astype(
            jnp.bfloat16
        ),
        "tp",
        scatter_dimension=0,
        tiled=True,
    )
    mix_output = mix_sum.T.astype(jnp.bfloat16)
    returning = expert_sum.reshape(feature_local, local_experts, ep_count, capacity)
    returned = lax.all_to_all(returning, "ep", split_axis=2, concat_axis=2, tiled=True)
    returned = returned.reshape(feature_local, local_experts * slot_rows)
    picked = lax.dot_general(
        returned, back_table, (((1,), (1,)), ((), ())), preferred_element_type=jnp.float32
    ).reshape(feature_local, tok_local, top_count)
    normalized = route_weight / jnp.sum(route_weight, axis=1, keepdims=True) * routed_scale
    expert_output = jnp.sum(picked * normalized[None], axis=2).T.astype(jnp.bfloat16)
    return (mix_output, expert_output)


def solution(mesh):
    in_specs = (
        P("ep", "tp"),
        P(),
        P(None, "tp"),
        P(None, "tp"),
        P(None, "tp"),
        P(None, "tp"),
        P("tp", None),
        P("ep", "tp"),
        P(),
        P("ep", None),
        P("ep", None),
        P("ep", None, "tp"),
        P("ep", None, "tp"),
        P("ep", "tp", None),
    )
    out_specs = (P("ep", "tp"), P("ep", "tp"))
    return jax.shard_map(local, mesh=mesh, in_specs=in_specs, out_specs=out_specs, check_vma=False)
```

profile of v0, /device:TPU:0, one launch (start us, length us, event | category | flops | bytes accessed | tf_op | source)
XLA Modules:
  0.0 158.1 jit_solution(9475336010663980682)
XLA Ops:
  7.2 0.9 copy.20
  8.3 0.9 reduce-window.6
  9.6 1.1 broadcast_in_dim.2
  10.7 0.8 reshape.158
  11.5 1.6 %convolution_convert_fusion.2 = bf16[640,512]{1,0:T(8,128)(2,1)S(1)} fusion(bf16[320,512]{1,0:T(8,128)(2,1)} %reshape.158, s32[320]{0:T(512)S(1)} %multiply_add_fusion), kind=kOutput, calls=%fused_computation.18 | convolution fusion | flops 210247680 | bytes 984320 | tf_op jit(solution)/shard_map/dot_general | solution.py:68
  13.1 24.9 %all_to_all.14 = bf16[8,1,80,512]{3,2,1,0:T(8,128)(2,1)} all-to-all(bf16[8,1,80,512]{3,2,1,0:T(8,128)(2,1)S(1)} %bitcast.51), channel_id=1, replica_groups=mesh['ep'=8,'tp'=4] {'ep'}, dimensions={0} | all-to-all | bytes 1310720 | tf_op jit(solution)/shard_map/all_to_all | solution.py:72
  38.1 0.7 all-gather.3.cloned.1.call-update
  38.8 23.6 %all-gather.5.cloned.1.call-done = bf16[640,2048]{1,0:T(8,128)(2,1)} async-done(((bf16[640,512]{1,0:T(8,128)(2,1)}), bf16[640,2048]{1,0:T(8,128)(2,1)}) %all-gather.5.cloned.1.call-update) | async-done | bytes 2621456 | tf_op jit(solution)/shard_map/all_gather | solution.py:80
  62.4 2.5 %fusion.1 = f32[640]{0:T(1024)S(1)} fusion(bf16[640,2048]{1,0:T(8,128)(2,1)} %all-gather.5.cloned.1.call-done), kind=kLoop, calls=%fused_computation.3 | loop fusion | flops 3931520 | bytes 2624000 | tf_op jit(solution)/shard_map/reduce_sum | solution.py:27
  64.9 5.4 %fusion.5 = f32[640,768]{1,0:T(8,128)} fusion(bf16[1,2048,768]{2,1,0:T(8,128)(2,1)} %param.26, bf16[640,2048]{1,0:T(8,128)(2,1)S(1)} %copy-done.1, f32[2048]{0:T(1024)S(1)} %copy-done.7), kind=kOutput, calls=%fused_computation.10 | convolution fusion | flops 2017198080 | bytes 7741440 | tf_op jit(solution)/shard_map/gsd,gdf->gsf/dot_general | solution.py:23
  70.4 10.0 %fusion.9 = bf16[2048,640]{0,1:T(8,128)(2,1)} fusion(bf16[1,768,2048]{2,1,0:T(8,128)(2,1)S(1)} %copy-done, f32[640,768]{1,0:T(8,128)} %fusion.5, bf16[1,2048,768]{2,1,0:T(8,128)(2,1)} %param.25, bf16[640,2048]{1,0:T(8,128)(2,1)} %all-gather.5.cloned.1.call-done, f32[2048]{0:T(1024)S(1)} %copy-done.7, f32[640]{0:T(1024)S(1)} %add_rsqrt_fusion), kind=kOutput, calls=%fused_computation.14 | convolution fusion | flops 4035706880 | bytes 13511168 | tf_op jit(solution)/shard_map/gsf,gfd->dgs/dot_general | solution.py:114
  80.4 3.2 %all-gather.3.cloned.1.call-done = bf16[384,2048]{1,0:T(8,128)(2,1)} async-done(((bf16[384,512]{1,0:T(8,128)(2,1)}), bf16[384,2048]{1,0:T(8,128)(2,1)}) %all-gather.3.cloned.1.call-update) | async-done | bytes 1572880 | tf_op jit(solution)/shard_map/all_gather | solution.py:77
  83.6 1.8 %fusion.3 = f32[384]{0:T(512)S(1)} fusion(bf16[384,2048]{1,0:T(8,128)(2,1)} %all-gather.3.cloned.1.call-done), kind=kLoop, calls=%fused_computation.8 | loop fusion | flops 2358912 | bytes 1574400 | tf_op jit(solution)/shard_map/reduce_sum | solution.py:27
  85.5 3.2 %convolution_multiply_fusion = f32[384,512]{1,0:T(8,128)S(1)} fusion(bf16[2048,512]{1,0:T(8,128)(2,1)} %param.18, bf16[384,2048]{1,0:T(8,128)(2,1)} %all-gather.3.cloned.1.call-done, f32[2048]{0:T(1024)S(1)} %copy-done.8, f32[384]{0:T(512)S(1)} %add_rsqrt_fusion.1), kind=kOutput, calls=%fused_computation.19 | convolution fusion | flops 807862272 | bytes 4466176 | tf_op jit(solution)/shard_map/gsd,gdf->gsf/dot_general | solution.py:23
  88.7 1.0 fusion.19
  89.7 3.4 %collective-permute-start = (f32[2,512]{1,0:T(2,128)S(1)}, f32[2,512]{1,0:T(2,128)S(1)}, u32[]{:S(2)}, u32[]{:S(2)}) collective-permute-start(f32[2,512]{1,0:T(2,128)S(1)} %slice.36), channel_id=1, source_target_pairs={{0,4},{4,8},{8,12},{12,16},{16,20},{20,24},{24,28},{1,5},{5,9},{9,... | collective-permute-start | bytes 12296 | tf_op jit(solution)/shard_map/ppermute | solution.py:13
  93.1 1.3 collective-permute-done
  94.4 6.7 %fusion.12 = bf16[2048,384]{0,1:T(8,128)(2,1)} fusion(bf16[512,2048]{1,0:T(8,128)(2,1)} %param.20, f32[2,512]{1,0:T(2,128)S(1)} %collective-permute-done, f32[384,512]{1,0:T(8,128)} %copy-done.5, bf16[2048,512]{1,0:T(8,128)(2,1)} %param.16, bf16[384,2048]{1,0:T(8,128)(2,1)} %all-gather.3.cloned.1.call-done, f32[2048]{0:T(1024)S(1)} %copy-done.8, ...), kind=kOutput, calls=%fused_computation.16 | convolution fusion | flops 1615724544 | bytes 8146432 | tf_op jit(solution)/shard_map/dot_general | solution.py:106
  101.2 19.4 %reduce-scatter.5.cloned.1.call-done = bf16[512,640]{0,1:T(8,128)(2,1)} async-done(((bf16[2048,640]{0,1:T(8,128)(2,1)}), bf16[512,640]{0,1:T(8,128)(2,1)}) %reduce-scatter.5.cloned.1.call-update) | async-done | bytes 655376 | tf_op jit(solution)/shard_map/reduce_scatter | solution.py:115
  120.6 5.5 %all-to-all-start.1 = ((bf16[512,1,8,80]{0,3,1,2:T(8,128)(2,1)}), bf16[512,1,8,80]{0,3,1,2:T(8,128)(2,1)}, u32[]{:S(2)}, u32[]{:S(2)}) async-start(bf16[512,1,8,80]{0,3,1,2:T(8,128)(2,1)} %bitcast.50), calls=%async_computation.3 | async-start | bytes 1310720 | tf_op jit(solution)/shard_map/all_to_all | solution.py:125
  126.3 1.0 eq.43
  127.3 16.0 %all-to-all-done.1 = bf16[512,1,8,80]{0,3,1,2:T(8,128)(2,1)} async-done(((bf16[512,1,8,80]{0,3,1,2:T(8,128)(2,1)}), bf16[512,1,8,80]{0,3,1,2:T(8,128)(2,1)}, u32[]{:S(2)}, u32[]{:S(2)}) %all-to-all-start.1) | async-done | bytes 655392 | tf_op jit(solution)/shard_map/all_to_all | solution.py:125
  143.3 2.3 %fusion.20 = bf16[512,160]{0,1:T(8,128)(2,1)} fusion(bf16[512,640,1]{0,1,2:T(8,128)(2,1)} %bitcast.18, pred[160,2,640]{2,1,0:T(4,128)(4,1)} %eq.43, f32[160,2]{0,1:T(2,128)S(1)} %divide_multiply_fusion), kind=kOutput, calls=%fused_computation.24 | convolution fusion | flops 209960960 | bytes 1025280 | tf_op jit(solution)/shard_map/dot_general | solution.py:127
  145.7 5.9 %reduce-scatter.3.cloned.1.call-done = bf16[512,384]{0,1:T(8,128)(2,1)} async-done(((bf16[2048,384]{0,1:T(8,128)(2,1)}), bf16[512,384]{0,1:T(8,128)(2,1)}) %reduce-scatter.3.cloned.1.call-update) | async-done | bytes 393232 | tf_op jit(solution)/shard_map/reduce_scatter | solution.py:105
  (40 shorter events, 1.0 us)
Async XLA Ops:
  7.2 63.2 %copy-start = (bf16[1,768,2048]{2,1,0:T(8,128)(2,1)S(1)}, bf16[1,768,2048]{2,1,0:T(8,128)(2,1)}, u32[]{:S(2)}) copy-start(bf16[1,768,2048]{2,1,0:T(8,128)(2,1)} %param.27) | copy-start | bytes 9437188
  7.2 55.2 %all-gather.5.cloned.1.call-start = ((), (), s32[]{:S(2)}) async-start(), calls=%async_computation.6 | async-start | bytes 3276800 | tf_op jit(solution)/shard_map/all_gather | solution.py:80
  38.0 26.9 %copy-start.7 = (f32[2048]{0:T(1024)S(1)}, f32[2048]{0:T(1024)}, u32[]{:S(2)}) copy-start(f32[2048]{0:T(1024)} %param.22) | copy-start | bytes 24580
  38.0 45.6 %all-gather.3.cloned.1.call-start = ((), (), s32[]{:S(2)}) async-start(), calls=%async_computation.4 | async-start | bytes 1966080 | tf_op jit(solution)/shard_map/all_gather | solution.py:77
  38.8 81.8 %reduce-scatter.5.cloned.1.call-start = ((), (), s32[]{:S(2)}) async-start(), calls=%async_computation.7 | async-start | bytes 3276800 | tf_op jit(solution)/shard_map/reduce_scatter | solution.py:115
  62.4 2.5 %copy-start.1 = (bf16[640,2048]{1,0:T(8,128)(2,1)S(1)}, bf16[640,2048]{1,0:T(8,128)(2,1)}, u32[]{:S(2)}) copy-start(bf16[640,2048]{1,0:T(8,128)(2,1)} %all-gather.5.cloned.1.call-done) | copy-start | bytes 7864324
  80.4 5.1 %copy-start.8 = (f32[2048]{0:T(1024)S(1)}, f32[2048]{0:T(1024)}, u32[]{:S(2)}) copy-start(f32[2048]{0:T(1024)} %param.15) | copy-start | bytes 24580
  80.4 71.2 %reduce-scatter.3.cloned.1.call-start = ((), (), s32[]{:S(2)}) async-start(), calls=%async_computation.5 | async-start | bytes 1966080 | tf_op jit(solution)/shard_map/reduce_scatter | solution.py:105
  85.4 3.2 %copy-start.2 = (bf16[384,2048]{1,0:T(8,128)(2,1)S(1)}, bf16[384,2048]{1,0:T(8,128)(2,1)}, u32[]{:S(2)}) copy-start(bf16[384,2048]{1,0:T(8,128)(2,1)} %all-gather.3.cloned.1.call-done) | copy-start | bytes 4718596
  85.4 3.2 %copy-start.6 = (bf16[2048,512]{1,0:T(8,128)(2,1)S(1)}, bf16[2048,512]{1,0:T(8,128)(2,1)}, u32[]{:S(2)}) copy-start(bf16[2048,512]{1,0:T(8,128)(2,1)} %param.17) | copy-start | bytes 6291460
  88.7 4.4 %copy-start.4 = (f32[3,512]{1,0:T(4,128)S(1)}, f32[3,512]{1,0:T(4,128)}, u32[]{:S(2)}) copy-start(f32[3,512]{1,0:T(4,128)} %param.19) | copy-start | bytes 18436
  89.7 4.7 %copy-start.5 = (f32[384,512]{1,0:T(8,128)}, f32[384,512]{1,0:T(8,128)S(1)}, u32[]{:S(2)}) copy-start(f32[384,512]{1,0:T(8,128)S(1)} %fusion.19) | copy-start | bytes 2359300
  89.7 4.7 %collective-permute-start = (f32[2,512]{1,0:T(2,128)S(1)}, f32[2,512]{1,0:T(2,128)S(1)}, u32[]{:S(2)}, u32[]{:S(2)}) collective-permute-start(f32[2,512]{1,0:T(2,128)S(1)} %slice.36), channel_id=1, source_target_pairs={{0,4},{4,8},{8,12},{12,16},{16,20},{20,24},{24,28},{1,5},{5,9},{9,... | collective-permute-start | bytes 12296 | tf_op jit(solution)/shard_map/ppermute | solution.py:13
  101.2 26.1 %copy-start.3 = (f32[160,2]{0,1:T(2,128)S(1)}, f32[160,2]{0,1:T(2,128)}, u32[]{:S(2)}) copy-start(f32[160,2]{0,1:T(2,128)} %param.24) | copy-start | bytes 3844
  120.6 22.7 %all-to-all-start.1 = ((bf16[512,1,8,80]{0,3,1,2:T(8,128)(2,1)}), bf16[512,1,8,80]{0,3,1,2:T(8,128)(2,1)}, u32[]{:S(2)}, u32[]{:S(2)}) async-start(bf16[512,1,8,80]{0,3,1,2:T(8,128)(2,1)} %bitcast.50), calls=%async_computation.3 | async-start | bytes 1310720 | tf_op jit(solution)/shard_map/all_to_all | solution.py:125
Sparse Core Ops, SparseCore 0:
  38.1 24.2 all-gather.4
  64.0 19.6 all-gather.2
  86.2 34.3 reduce-scatter.4
  123.5 27.9 reduce-scatter.2
where the time goes:
time: 158 us
  waiting for transfers between devices  70.1 us (44%)
  matrix products  30.3 us (19%)
  blocking collectives  24.9 us (16%)
  between operations  13.9 us (9%)
  starting transfers between devices  9.05 us (6%)
  other arithmetic  5.51 us (3%)
  local copies, waits for them, and re-layouts  4.3 us (3%)
    all_to_all x1, blocking collectives, local(): lax.all_to_all(outgoing, 'ep', split_axis=0, concat_axis=2, tiled=True)  24.9 us
    all_gather x1, waiting for transfers between devices, local(): lax.all_gather(arrived, 'tp', axis=1, tiled=True)  23.6 us
    reduce_scatter x1, waiting for transfers between devices, local(): lax.psum_scatter(summed.reshape(lax.axis_size('tp') * feature_local, loca...  19.4 us
    all_to_all x1, waiting for transfers between devices, local(): lax.all_to_all(returning, 'ep', split_axis=2, concat_axis=2, tiled=True)  16 us
    dot_general x1, matrix products, local(): jnp.einsum('gsf,gfd->dgs', activated, sliced, preferred_element_type=jnp....  9.98 us
    dot_general x3, matrix products, project_piece(): jnp.einsum('gsd,gdf->gsf', grouped, matrix, preferred_element_type=jnp.fl...  9.62 us
    dot_general x1, matrix products, local(): lax.dot_general(sliced, gated, (((0,), (1,)), ((), ())), preferred_elemen...  6.74 us
    reduce_scatter x1, waiting for transfers between devices, local(): lax.psum_scatter(lax.dot_general(sliced, gated, (((0,), (1,)), ((), ())),...  5.88 us
  transfers between devices with their start and end apart: 6, of which 6 were waited for; matrix products, arithmetic and copies ran while one was open for 22% of the time, Pallas kernels for 0%

commit v1 on v0

--- a/solution.py
+++ b/solution.py
@@ -5,6 +5,17 @@
 
 epsilon = 1e-06
 routed_scale = 2.5
+
+
+def in_blocks(x, dim, size):
+    before, after = (x.shape[:dim], x.shape[dim + 1 :])
+    return jnp.moveaxis(x.reshape(*before, size, -1, *after), dim, 0)
+
+
+def laid_out(blocks, dim):
+    blocks = jnp.moveaxis(blocks, 0, dim)
+    dims = blocks.shape
+    return blocks.reshape(*dims[:dim], dims[dim] * dims[dim + 1], *dims[dim + 2 :])
 
 
 def passed_along(block, axis, distance):
@@ -69,7 +80,15 @@
         send_table, repeated, (((0,), (0,)), ((), ())), preferred_element_type=jnp.float32
     ).astype(jnp.bfloat16)
     outgoing = outgoing.reshape(ep_count, local_experts, capacity, feature_local)
-    arrived = lax.all_to_all(outgoing, "ep", split_axis=0, concat_axis=2, tiled=True)
+    size, index = (lax.axis_size("ep"), lax.axis_index("ep"))
+    blocks = in_blocks(outgoing, 0, size)
+    whole = blocks
+    for step in range(1, size):
+        target, source = ((index + step) % size, (index - step) % size)
+        sent = lax.dynamic_index_in_dim(blocks, target, 0)
+        other = lax.ppermute(sent, "ep", [(i_2, (i_2 + step) % size) for i_2 in range(size)])
+        whole = lax.dynamic_update_slice_in_dim(whole, other, source, axis=0)
+    arrived = laid_out(whole, 2)
     arrived = arrived.reshape(local_experts * slot_rows, feature_local)
     mix_weights = (gate_b_weight[None], gate_c_weight[None], value_weight[None])
     expert_weights = (expert_gate, expert_up)

time: 158 us -> 164 us (1.038)
  blocking collectives: 24.9 us -> 0 us
  starting transfers between devices: 9.05 us -> 20.4 us
  waiting for transfers between devices: 70.1 us -> 81.3 us
  local copies, waits for them, and re-layouts: 4.3 us -> 11.8 us
    all_to_all x1 -> x0, blocking collectives: 24.9 us -> none  [local(): lax.all_to_all(outgoing, 'ep', split_axis=0, concat_axis=2, tiled=True)]
    ppermute x0 -> x7, starting transfers between devices: none -> 11.2 us  [local(): lax.ppermute(sent, 'ep', [(i_2, (i_2 + step) % size) for i_2 in range(siz...]
    ppermute x0 -> x7, waiting for transfers between devices: none -> 8.04 us  [local(): lax.ppermute(sent, 'ep', [(i_2, (i_2 + step) % size) for i_2 in range(siz...]
    dynamic_update_slice x0 -> x6, local copies, waits for them, and re-layouts: none -> 4.73 us  [local(): whole = lax.dynamic_update_slice_in_dim(whole, other, source, axis=0)]
    all_gather x1, waiting for transfers between devices: 23.6 us -> 26.9 us  [local(): lax.all_gather(arrived, 'tp', axis=1, tiled=True)]
    dynamic_slice x0 -> x2, local copies, waits for them, and re-layouts: none -> 1.83 us  [local(): sent = lax.dynamic_index_in_dim(blocks, target, 0)]
  transfers between devices with their start and end apart: 6 -> 13, of which waited for: 6 -> 8; matrix products, arithmetic and copies ran while one was open for 22% -> 23% of each run, Pallas kernels for 0% -> 0%
where the time goes in v1:
time: 164 us; the launch traced here: 163 us
  waiting for transfers between devices  81.3 us (50%)
  matrix products  30.3 us (18%)
  starting transfers between devices  20.4 us (12%)
  between operations  14 us (9%)
  local copies, waits for them, and re-layouts  11.8 us (7%)
  other arithmetic  5.51 us (3%)
    all_gather x1, waiting for transfers between devices, local(): lax.all_gather(arrived, 'tp', axis=1, tiled=True)  26.9 us
    reduce_scatter x1, waiting for transfers between devices, local(): lax.psum_scatter(summed.reshape(lax.axis_size('tp') * feature_local, loca...  19.4 us
    all_to_all x1, waiting for transfers between devices, local(): lax.all_to_all(returning, 'ep', split_axis=2, concat_axis=2, tiled=True)  16 us
    ppermute x7, starting transfers between devices, local(): lax.ppermute(sent, 'ep', [(i_2, (i_2 + step) % size) for i_2 in range(siz...  11.2 us
    dot_general x1, matrix products, local(): jnp.einsum('gsf,gfd->dgs', activated, sliced, preferred_element_type=jnp....  9.97 us
    dot_general x3, matrix products, project_piece(): jnp.einsum('gsd,gdf->gsf', grouped, matrix, preferred_element_type=jnp.fl...  9.64 us
    ppermute x7, waiting for transfers between devices, local(): lax.ppermute(sent, 'ep', [(i_2, (i_2 + step) % size) for i_2 in range(siz...  8.04 us
    dot_general x1, matrix products, local(): lax.dot_general(sliced, gated, (((0,), (1,)), ((), ())), preferred_elemen...  6.75 us
  transfers between devices with their start and end apart: 13, of which 8 were waited for; matrix products, arithmetic and copies ran while one was open for 23% of the time, Pallas kernels for 0%

profile of v1, /device:TPU:0, one launch (start us, length us, event | category | flops | bytes accessed | tf_op | source)
XLA Modules:
  0.0 163.2 jit_solution(13776471515225128158)
XLA Ops:
  11.5 1.6 convolution_convert_fusion.2
  14.0 3.0 %collective-permute-start.1 = (bf16[1,1,1,80,512]{4,3,0,2,1:T(8,128)(2,1)S(1)}, bf16[1,1,1,80,512]{4,3,0,2,1:T(8,128)(2,1)}, u32[]{:S(2)}, u32[]{:S(2)}) collective-permute-start(bf16[1,1,1,80,512]{4,3,0,2,1:T(8,128)(2,1)S(1)} %constant_dynamic-slice_fusion.6), channel_id=1, source_target_pairs={{0,4},{4,8},{8,12},{12,16},{16,20},{20,24},{24,28},{28,0},{1,5},{5... | collective-permute-start | bytes 245768 | tf_op jit(solution)/shard_map/ppermute | solution.py:89
  17.0 5.6 %collective-permute-done.1 = bf16[1,1,1,80,512]{4,3,0,2,1:T(8,128)(2,1)} collective-permute-done((bf16[1,1,1,80,512]{4,3,0,2,1:T(8,128)(2,1)S(1)}, bf16[1,1,1,80,512]{4,3,0,2,1:T(8,128)(2,1)}, u32[]{:S(2)}, u32[]{:S(2)}) %collective-permute-start.1) | collective-permute-done | bytes 81952 | tf_op jit(solution)/shard_map/ppermute | solution.py:89
  22.6 1.8 %constant_dynamic-slice_fusion = (bf16[1,1,1,80,512]{4,3,0,2,1:T(8,128)(2,1)S(1)}, bf16[1,1,1,80,512]{4,3,0,2,1:T(8,128)(2,1)S(1)}, bf16[1,1,1,80,512]{4,3,0,2,1...) fusion(bf16[8,1,1,80,512]{4,3,0,2,1:T(8,128)(2,1)} %bitcast.48,, ...), kind=kLoop, calls=%fused_computation.54 | loop fusion | bytes 1146908 | tf_op jit(solution)/shard_map/jit(dynamic_index_in_dim)/dynamic_slice | solution.py:88
  24.4 1.5 collective-permute-start.3
  26.0 1.2 collective-permute-start.4
  27.2 3.6 %collective-permute-start.5 = (bf16[1,1,1,80,512]{4,3,0,2,1:T(8,128)(2,1)S(1)}, bf16[1,1,1,80,512]{4,3,0,2,1:T(8,128)(2,1)S(1)}, u32[]{:S(2)}, u32[]{:S(2)}) collective-permute-start(bf16[1,1,1,80,512]{4,3,0,2,1:T(8,128)(2,1)S(1)} %get-tuple-element.4), channel_id=1, source_target_pairs={{0,20},{4,24},{8,28},{12,0},{16,4},{20,8},{24,12},{28,16},{1,21},{... | collective-permute-start | bytes 245768 | tf_op jit(solution)/shard_map/ppermute | solution.py:89
  30.8 1.3 collective-permute-start.6
  32.6 1.5 constant_dynamic-update-slice_fusion.5
  34.8 2.4 %collective-permute-done.4 = bf16[1,1,1,80,512]{4,3,0,2,1:T(8,128)(2,1)S(1)} collective-permute-done((bf16[1,1,1,80,512]{4,3,0,2,1:T(8,128)(2,1)S(1)}, bf16[1,1,1,80,512]{4,3,0,2,1:T(8,128)(2,1)S(1)}, u32[]{:S(2)}, u32[]{:S(2)}) %collective-permute-start.4) | collective-permute-done | bytes 81952 | tf_op jit(solution)/shard_map/ppermute | solution.py:89
  40.6 26.9 %all-gather.5.cloned.1.call-done = bf16[640,2048]{1,0:T(8,128)(2,1)} async-done(((bf16[640,512]{1,0:T(8,128)(2,1)}), bf16[640,2048]{1,0:T(8,128)(2,1)}) %all-gather.5.cloned.1.call-update) | async-done | bytes 2621456 | tf_op jit(solution)/shard_map/all_gather | solution.py:99
  67.5 2.5 %fusion.1 = f32[640]{0:T(1024)S(1)} fusion(bf16[640,2048]{1,0:T(8,128)(2,1)} %all-gather.5.cloned.1.call-done), kind=kLoop, calls=%fused_computation.3 | loop fusion | flops 3931520 | bytes 2624000 | tf_op jit(solution)/shard_map/reduce_sum | solution.py:38
  70.1 5.4 %fusion.7 = f32[640,768]{1,0:T(8,128)} fusion(bf16[1,2048,768]{2,1,0:T(8,128)(2,1)} %param.25, bf16[640,2048]{1,0:T(8,128)(2,1)S(1)} %copy-done.1, f32[2048]{0:T(1024)S(1)} %copy-done.10), kind=kOutput, calls=%fused_computation.12 | convolution fusion | flops 2017198080 | bytes 7741440 | tf_op jit(solution)/shard_map/gsd,gdf->gsf/dot_general | solution.py:34
  75.5 10.0 %fusion.9 = bf16[2048,640]{0,1:T(8,128)(2,1)} fusion(bf16[1,768,2048]{2,1,0:T(8,128)(2,1)S(1)} %copy-done, f32[640,768]{1,0:T(8,128)} %fusion.7, bf16[1,2048,768]{2,1,0:T(8,128)(2,1)} %param.26, bf16[640,2048]{1,0:T(8,128)(2,1)} %all-gather.5.cloned.1.call-done, f32[2048]{0:T(1024)S(1)} %copy-done.10, f32[640]{0:T(1024)S(1)} %add_rsqrt_fusion), kind=kOutput, calls=%fused_computation.14 | convolution fusion | flops 4035706880 | bytes 13511168 | tf_op jit(solution)/shard_map/gsf,gfd->dgs/dot_general | solution.py:133
  85.6 3.2 %all-gather.3.cloned.1.call-done = bf16[384,2048]{1,0:T(8,128)(2,1)} async-done(((bf16[384,512]{1,0:T(8,128)(2,1)}), bf16[384,2048]{1,0:T(8,128)(2,1)}) %all-gather.3.cloned.1.call-update) | async-done | bytes 1572880 | tf_op jit(solution)/shard_map/all_gather | solution.py:96
  88.8 1.8 %fusion.3 = f32[384]{0:T(512)S(1)} fusion(bf16[384,2048]{1,0:T(8,128)(2,1)} %all-gather.3.cloned.1.call-done), kind=kLoop, calls=%fused_computation.8 | loop fusion | flops 2358912 | bytes 1574400 | tf_op jit(solution)/shard_map/reduce_sum | solution.py:38
  90.6 3.2 %convolution_multiply_fusion = f32[384,512]{1,0:T(8,128)S(1)} fusion(bf16[2048,512]{1,0:T(8,128)(2,1)} %param.18, bf16[384,2048]{1,0:T(8,128)(2,1)} %all-gather.3.cloned.1.call-done, f32[2048]{0:T(1024)S(1)} %copy-done.11, f32[384]{0:T(512)S(1)} %add_rsqrt_fusion.1), kind=kOutput, calls=%fused_computation.19 | convolution fusion | flops 807862272 | bytes 4466176 | tf_op jit(solution)/shard_map/gsd,gdf->gsf/dot_general | solution.py:34
  94.9 3.5 %collective-permute-start = (f32[2,512]{1,0:T(2,128)S(1)}, f32[2,512]{1,0:T(2,128)S(1)}, u32[]{:S(2)}, u32[]{:S(2)}) collective-permute-start(f32[2,512]{1,0:T(2,128)S(1)} %slice.36), channel_id=1, source_target_pairs={{0,4},{4,8},{8,12},{12,16},{16,20},{20,24},{24,28},{1,5},{5,9},{9,... | collective-permute-start | bytes 12296 | tf_op jit(solution)/shard_map/ppermute | solution.py:24
  99.6 6.7 %fusion.12 = bf16[2048,384]{0,1:T(8,128)(2,1)} fusion(bf16[512,2048]{1,0:T(8,128)(2,1)} %param.20, f32[2,512]{1,0:T(2,128)S(1)} %collective-permute-done, f32[384,512]{1,0:T(8,128)} %copy-done.8, bf16[2048,512]{1,0:T(8,128)(2,1)} %param.16, bf16[384,2048]{1,0:T(8,128)(2,1)} %all-gather.3.cloned.1.call-done, f32[2048]{0:T(1024)S(1)} %copy-done.11, ...), kind=kOutput, calls=%fused_computation.16 | convolution fusion | flops 1615724544 | bytes 8146432 | tf_op jit(solution)/shard_map/dot_general | solution.py:125
  106.3 19.4 %reduce-scatter.5.cloned.1.call-done = bf16[512,640]{0,1:T(8,128)(2,1)} async-done(((bf16[2048,640]{0,1:T(8,128)(2,1)}), bf16[512,640]{0,1:T(8,128)(2,1)}) %reduce-scatter.5.cloned.1.call-update) | async-done | bytes 655376 | tf_op jit(solution)/shard_map/reduce_scatter | solution.py:134
  125.7 5.5 %all-to-all-start = ((bf16[512,1,8,80]{0,3,1,2:T(8,128)(2,1)}), bf16[512,1,8,80]{0,3,1,2:T(8,128)(2,1)}, u32[]{:S(2)}, u32[]{:S(2)}) async-start(bf16[512,1,8,80]{0,3,1,2:T(8,128)(2,1)} %bitcast.50), calls=%async_computation.2 | async-start | bytes 1310720 | tf_op jit(solution)/shard_map/all_to_all | solution.py:144
  132.5 16.0 %all-to-all-done = bf16[512,1,8,80]{0,3,1,2:T(8,128)(2,1)} async-done(((bf16[512,1,8,80]{0,3,1,2:T(8,128)(2,1)}), bf16[512,1,8,80]{0,3,1,2:T(8,128)(2,1)}, u32[]{:S(2)}, u32[]{:S(2)}) %all-to-all-start) | async-done | bytes 655392 | tf_op jit(solution)/shard_map/all_to_all | solution.py:144
  148.5 2.3 %fusion.20 = bf16[512,160]{0,1:T(8,128)(2,1)} fusion(bf16[512,640,1]{0,1,2:T(8,128)(2,1)} %bitcast.17, pred[160,2,640]{2,1,0:T(4,128)(4,1)} %eq.58, f32[160,2]{0,1:T(2,128)S(1)} %divide_multiply_fusion), kind=kOutput, calls=%fused_computation.24 | convolution fusion | flops 209960960 | bytes 1025280 | tf_op jit(solution)/shard_map/dot_general | solution.py:146
  150.8 5.9 %reduce-scatter.3.cloned.1.call-done = bf16[512,384]{0,1:T(8,128)(2,1)} async-done(((bf16[2048,384]{0,1:T(8,128)(2,1)}), bf16[512,384]{0,1:T(8,128)(2,1)}) %reduce-scatter.3.cloned.1.call-update) | async-done | bytes 393232 | tf_op jit(solution)/shard_map/reduce_scatter | solution.py:124
  (67 shorter events, 13.2 us)
Async XLA Ops:
  7.2 68.4 %copy-start = (bf16[1,768,2048]{2,1,0:T(8,128)(2,1)S(1)}, bf16[1,768,2048]{2,1,0:T(8,128)(2,1)}, u32[]{:S(2)}) copy-start(bf16[1,768,2048]{2,1,0:T(8,128)(2,1)} %param.27) | copy-start | bytes 9437188
  7.2 60.4 %all-gather.5.cloned.1.call-start = ((), (), s32[]{:S(2)}) async-start(), calls=%async_computation.5 | async-start | bytes 3276800 | tf_op jit(solution)/shard_map/all_gather | solution.py:99
  9.6 7.4 %copy-start.4 = (s32[320]{0:T(512)}, s32[320]{0:T(512)S(1)}, u32[]{:S(2)}) copy-start(s32[320]{0:T(512)S(1)} %multiply_add_fusion) | copy-start | bytes 3844
  14.0 8.6 %collective-permute-start.1 = (bf16[1,1,1,80,512]{4,3,0,2,1:T(8,128)(2,1)S(1)}, bf16[1,1,1,80,512]{4,3,0,2,1:T(8,128)(2,1)}, u32[]{:S(2)}, u32[]{:S(2)}) collective-permute-start(bf16[1,1,1,80,512]{4,3,0,2,1:T(8,128)(2,1)S(1)} %constant_dynamic-slice_fusion.6), channel_id=1, source_target_pairs={{0,4},{4,8},{8,12},{12,16},{16,20},{20,24},{24,28},{28,0},{1,5},{5... | collective-permute-start | bytes 245768 | tf_op jit(solution)/shard_map/ppermute | solution.py:89
  24.4 7.7 %collective-permute-start.2 = (bf16[1,1,1,80,512]{4,3,0,2,1:T(8,128)(2,1)}, bf16[1,1,1,80,512]{4,3,0,2,1:T(8,128)(2,1)}, u32[]{:S(2)}, u32[]{:S(2)}) collective-permute-start(bf16[1,1,1,80,512]{4,3,0,2,1:T(8,128)(2,1)} %get-tuple-element.7), channel_id=1, source_target_pairs={{0,8},{4,12},{8,16},{12,20},{16,24},{20,28},{24,0},{28,4},{1,9},{5... | collective-permute-start | bytes 245768 | tf_op jit(solution)/shard_map/ppermute | solution.py:89
  24.4 9.7 %collective-permute-start.3 = (bf16[1,1,1,80,512]{4,3,0,2,1:T(8,128)(2,1)S(1)}, bf16[1,1,1,80,512]{4,3,0,2,1:T(8,128)(2,1)S(1)}, u32[]{:S(2)}, u32[]{:S(2)}) collective-permute-start(bf16[1,1,1,80,512]{4,3,0,2,1:T(8,128)(2,1)S(1)} %get-tuple-element.6), channel_id=1, source_target_pairs={{0,12},{4,16},{8,20},{12,24},{16,28},{20,0},{24,4},{28,8},{1,13},{... | collective-permute-start | bytes 245768 | tf_op jit(solution)/shard_map/ppermute | solution.py:89
  26.0 11.3 %collective-permute-start.4 = (bf16[1,1,1,80,512]{4,3,0,2,1:T(8,128)(2,1)S(1)}, bf16[1,1,1,80,512]{4,3,0,2,1:T(8,128)(2,1)S(1)}, u32[]{:S(2)}, u32[]{:S(2)}) collective-permute-start(bf16[1,1,1,80,512]{4,3,0,2,1:T(8,128)(2,1)S(1)} %get-tuple-element.5), channel_id=1, source_target_pairs={{0,16},{4,20},{8,24},{12,28},{16,0},{20,4},{24,8},{28,12},{1,17},{... | collective-permute-start | bytes 245768 | tf_op jit(solution)/shard_map/ppermute | solution.py:89
  27.2 10.7 %collective-permute-start.5 = (bf16[1,1,1,80,512]{4,3,0,2,1:T(8,128)(2,1)S(1)}, bf16[1,1,1,80,512]{4,3,0,2,1:T(8,128)(2,1)S(1)}, u32[]{:S(2)}, u32[]{:S(2)}) collective-permute-start(bf16[1,1,1,80,512]{4,3,0,2,1:T(8,128)(2,1)S(1)} %get-tuple-element.4), channel_id=1, source_target_pairs={{0,20},{4,24},{8,28},{12,0},{16,4},{20,8},{24,12},{28,16},{1,21},{... | collective-permute-start | bytes 245768 | tf_op jit(solution)/shard_map/ppermute | solution.py:89
  30.8 7.8 %collective-permute-start.6 = (bf16[1,1,1,80,512]{4,3,0,2,1:T(8,128)(2,1)S(1)}, bf16[1,1,1,80,512]{4,3,0,2,1:T(8,128)(2,1)S(1)}, u32[]{:S(2)}, u32[]{:S(2)}) collective-permute-start(bf16[1,1,1,80,512]{4,3,0,2,1:T(8,128)(2,1)S(1)} %get-tuple-element.3), channel_id=1, source_target_pairs={{0,24},{4,28},{8,0},{12,4},{16,8},{20,12},{24,16},{28,20},{1,25},{... | collective-permute-start | bytes 245768 | tf_op jit(solution)/shard_map/ppermute | solution.py:89
  32.1 7.1 %collective-permute-start.7 = (bf16[1,1,1,80,512]{4,3,0,2,1:T(8,128)(2,1)S(1)}, bf16[1,1,1,80,512]{4,3,0,2,1:T(8,128)(2,1)S(1)}, u32[]{:S(2)}, u32[]{:S(2)}) collective-permute-start(bf16[1,1,1,80,512]{4,3,0,2,1:T(8,128)(2,1)S(1)} %get-tuple-element.2), channel_id=1, source_target_pairs={{0,28},{4,0},{8,4},{12,8},{16,12},{20,16},{24,20},{28,24},{1,29},{... | collective-permute-start | bytes 245768 | tf_op jit(solution)/shard_map/ppermute | solution.py:89
  37.9 32.1 %copy-start.10 = (f32[2048]{0:T(1024)S(1)}, f32[2048]{0:T(1024)}, u32[]{:S(2)}) copy-start(f32[2048]{0:T(1024)} %param.22) | copy-start | bytes 24580
  39.8 48.9 %all-gather.3.cloned.1.call-start = ((), (), s32[]{:S(2)}) async-start(), calls=%async_computation.3 | async-start | bytes 1966080 | tf_op jit(solution)/shard_map/all_gather | solution.py:96
  40.6 85.1 %reduce-scatter.5.cloned.1.call-start = ((), (), s32[]{:S(2)}) async-start(), calls=%async_computation.6 | async-start | bytes 3276800 | tf_op jit(solution)/shard_map/reduce_scatter | solution.py:134
  67.5 2.5 %copy-start.1 = (bf16[640,2048]{1,0:T(8,128)(2,1)S(1)}, bf16[640,2048]{1,0:T(8,128)(2,1)}, u32[]{:S(2)}) copy-start(bf16[640,2048]{1,0:T(8,128)(2,1)} %all-gather.5.cloned.1.call-done) | copy-start | bytes 7864324
  85.5 5.1 %copy-start.11 = (f32[2048]{0:T(1024)S(1)}, f32[2048]{0:T(1024)}, u32[]{:S(2)}) copy-start(f32[2048]{0:T(1024)} %param.15) | copy-start | bytes 24580
  85.5 71.2 %reduce-scatter.3.cloned.1.call-start = ((), (), s32[]{:S(2)}) async-start(), calls=%async_computation.4 | async-start | bytes 1966080 | tf_op jit(solution)/shard_map/reduce_scatter | solution.py:124
  90.6 3.2 %copy-start.3 = (bf16[384,2048]{1,0:T(8,128)(2,1)S(1)}, bf16[384,2048]{1,0:T(8,128)(2,1)}, u32[]{:S(2)}) copy-start(bf16[384,2048]{1,0:T(8,128)(2,1)} %all-gather.3.cloned.1.call-done) | copy-start | bytes 4718596
  90.6 3.2 %copy-start.9 = (bf16[2048,512]{1,0:T(8,128)(2,1)S(1)}, bf16[2048,512]{1,0:T(8,128)(2,1)}, u32[]{:S(2)}) copy-start(bf16[2048,512]{1,0:T(8,128)(2,1)} %param.17) | copy-start | bytes 6291460
  93.8 4.6 %copy-start.7 = (f32[3,512]{1,0:T(4,128)S(1)}, f32[3,512]{1,0:T(4,128)}, u32[]{:S(2)}) copy-start(f32[3,512]{1,0:T(4,128)} %param.19) | copy-start | bytes 18436
  94.8 4.7 %copy-start.8 = (f32[384,512]{1,0:T(8,128)}, f32[384,512]{1,0:T(8,128)S(1)}, u32[]{:S(2)}) copy-start(f32[384,512]{1,0:T(8,128)S(1)} %fusion.19) | copy-start | bytes 2359300
  94.9 4.7 %collective-permute-start = (f32[2,512]{1,0:T(2,128)S(1)}, f32[2,512]{1,0:T(2,128)S(1)}, u32[]{:S(2)}, u32[]{:S(2)}) collective-permute-start(f32[2,512]{1,0:T(2,128)S(1)} %slice.36), channel_id=1, source_target_pairs={{0,4},{4,8},{8,12},{12,16},{16,20},{20,24},{24,28},{1,5},{5,9},{9,... | collective-permute-start | bytes 12296 | tf_op jit(solution)/shard_map/ppermute | solution.py:24
  106.3 24.9 %copy-start.5 = (s32[320]{0:T(512)S(1)}, s32[320]{0:T(512)}, u32[]{:S(2)}) copy-start(s32[320]{0:T(512)} %copy-done.4) | copy-start | bytes 3844
  106.3 26.1 %copy-start.6 = (f32[160,2]{0,1:T(2,128)S(1)}, f32[160,2]{0,1:T(2,128)}, u32[]{:S(2)}) copy-start(f32[160,2]{0,1:T(2,128)} %param.24) | copy-start | bytes 3844
  125.7 22.7 %all-to-all-start = ((bf16[512,1,8,80]{0,3,1,2:T(8,128)(2,1)}), bf16[512,1,8,80]{0,3,1,2:T(8,128)(2,1)}, u32[]{:S(2)}, u32[]{:S(2)}) async-start(bf16[512,1,8,80]{0,3,1,2:T(8,128)(2,1)} %bitcast.50), calls=%async_computation.2 | async-start | bytes 1310720 | tf_op jit(solution)/shard_map/all_to_all | solution.py:144
  (1 other events, 0.9 us)
Sparse Core Ops, SparseCore 0:
  40.0 27.5 all-gather.4
  69.1 19.6 all-gather.2
  91.3 34.3 reduce-scatter.4
  128.7 27.9 reduce-scatter.2
